TPU v7x, 32 devices: a whole 2x2x4 slice. The times are simulated.
32 devices in a mesh: sp: 8 (over z, y), dp: 4 (over x, core).
Axes of the slice: x: 2, y: 2, z: 4, core: 2. Of those that a mesh axis runs over, the one named last changes fastest.
Arguments:
- skip_connection_stream: bfloat16 [4, 1024, 2048], P('dp', 'sp'), may hold values from -6 to 6
- emitted_valve_unscaled: bfloat16 [4, 1024, 1024], P('dp', 'sp'), may hold values from -6 to 6
- channel_source_mapped: bfloat16 [4, 1024, 1024], P('dp', 'sp'), may hold values from -6 to 6
- hidden_source_mapped: bfloat16 [4, 1024, 256], P('dp', 'sp'), may hold values from -6 to 6
- probe_mapped_values: bfloat16 [4, 1024, 256], P('dp', 'sp'), may hold values from -6 to 6
- increment_premapped: float32 [4, 1024, 16], P('dp', None, 'sp'), may hold values from -6 to 6
- extra_log_fading: float32 [4, 1024, 16], P('dp', None, 'sp'), may hold values from -2 to 0
- channel_fading_speed: float32 [16], replicated, may hold values from 0 to 1, as said below
- channel_source_kernel: float32 [4, 1024], replicated, may hold values from -3 to 3
- hidden_source_kernel: float32 [4, 256], replicated, may hold values from -3 to 3
- probe_kernel_coefficients: float32 [4, 256], replicated, may hold values from -3 to 3
- cluster_scaling_factor: float32 [1024], replicated, may hold values from 0.1 to 1.9
- emitted_mapping_matrix: bfloat16 [1024, 2048], replicated, may hold values from -0.1875 to 0.1875
- standardize_scaling: float32 [2048], replicated, may hold values from 0.1 to 1.9
- standardize_offset: float32 [2048], replicated, may hold values from -2 to 2
- chosen_specialist_ids: int32 [4, 1024, 2], P('dp', 'sp'), may hold values from 0 to 7, all different within a row; in each aligned block of 128 rows (0 to 127, 128 to 255, ..., all dimensions but the last counted through in order) at most 48 rows name the same one
- specialist_mixing_shares: float32 [4, 1024, 2], P('dp', 'sp'), may hold values from 0.2 to 1
- specialist_gating_matrices: bfloat16 [8, 2048, 5120], P('sp', None, 'dp'), may hold values from -0.125 to 0.125
- raising_matrices: bfloat16 [8, 2048, 5120], P('sp', None, 'dp'), may hold values from -0.125 to 0.125
- lowering_matrices: bfloat16 [8, 5120, 2048], P('sp', 'dp'), may hold values from -0.078125 to 0.078125
Outputs:
- layer_out: bfloat16 [4, 1024, 2048], P('dp', 'sp')
Inputs may be any that keep to these rules, and one draw needn't show every extreme that they name: `chosen_specialist_ids`: each row names two different experts. The rows of one device name no expert more than 48 times, a bound that some block reaches. `channel_fading_speed`: Positive.
All inputs are finite; a program needn't handle non-finite values.
Results may differ from a plain program's by a relative error of at most 0.015.
Values may be sent and summed in bfloat16 or wider, within the bound.
A program may use at most 128 MiB of HBM per device.

v0:
```python
import jax
import jax.numpy as jnp
from jax import lax
from jax.sharding import PartitionSpec as P

HEADS = 16
HEAD_DIM = 64
GROUPS = 4
STATE = 64
KERNEL = 4
BLK = 128


rms_eps = 1e-06
norm_eps = 1e-05


def causal_conv(series, tap_weights, rim_rows):
    padded = jnp.concatenate([rim_rows, series], axis=0).astype(jnp.float32)
    length = series.shape[0]
    running = jnp.zeros(series.shape, jnp.float32)
    for tap_index in range(tap_weights.shape[0]):
        running = running + tap_weights[tap_index] * lax.slice_in_dim(
            padded, tap_index, tap_index + length, axis=0
        )
    return jax.nn.silu(running).astype(jnp.bfloat16)


def ssd_blocks(x_conv, b_conv, c_conv, increment_delta, fading_exponent, init_state, block_len):
    length, head_count, head_width = x_conv.shape
    state_width = b_conv.shape[2]
    block_count = length // block_len
    x_block = x_conv.reshape(block_count, block_len, head_count, head_width)
    b_block = b_conv.reshape(block_count, block_len, head_count, state_width)
    c_block = c_conv.reshape(block_count, block_len, head_count, state_width)
    cumulative = jnp.cumsum(
        jnp.transpose(fading_exponent.reshape(block_count, block_len, head_count), (0, 2, 1)),
        axis=2,
    )
    step_heads = jnp.transpose(
        increment_delta.reshape(block_count, block_len, head_count), (0, 2, 1)
    )
    causal = jnp.arange(block_len)[:, None] >= jnp.arange(block_len)[None, :]
    within = jnp.exp(
        jnp.where(causal, cumulative[:, :, :, None] - cumulative[:, :, None, :], -jnp.inf)
    )
    scores = jnp.einsum("cthn,cshn->chts", c_block, b_block, preferred_element_type=jnp.float32)
    mixing = (scores * within * step_heads[:, :, None, :]).astype(jnp.bfloat16)
    diag_out = jnp.einsum("chts,cshp->cthp", mixing, x_block, preferred_element_type=jnp.float32)
    tail_decay = jnp.exp(cumulative[:, :, -1:] - cumulative) * step_heads
    scaled = (
        x_block.astype(jnp.float32) * jnp.transpose(tail_decay, (0, 2, 1))[:, :, :, None]
    ).astype(jnp.bfloat16)
    block_state = jnp.einsum("cshp,cshn->chpn", scaled, b_block, preferred_element_type=jnp.float32)
    totals = cumulative[:, :, -1]
    through = jnp.cumsum(totals, axis=0)
    before = through - totals
    earlier = jnp.arange(block_count)[:, None] > jnp.arange(block_count)[None, :]
    carry_weight = jnp.exp(
        jnp.where(earlier[:, :, None], before[:, None, :] - through[None, :, :], -jnp.inf)
    )
    entering = (
        jnp.einsum("cjh,jhpn->chpn", carry_weight, block_state, precision=lax.Precision.HIGHEST)
        + jnp.exp(before)[:, :, None, None] * init_state[None]
    )
    reach_decay = jnp.transpose(jnp.exp(cumulative), (0, 2, 1))
    carried_out = (
        jnp.einsum(
            "cthn,chpn->cthp",
            c_block.astype(jnp.float32),
            entering,
            precision=lax.Precision.HIGHEST,
        )
        * reach_decay[:, :, :, None]
    )
    outcome = (diag_out + carried_out).reshape(length, head_count, head_width)
    final_state = (
        jnp.einsum(
            "jh,jhpn->hpn",
            jnp.exp(through[-1][None, :] - through),
            block_state,
            precision=lax.Precision.HIGHEST,
        )
        + jnp.exp(through[-1])[:, None, None] * init_state
    )
    return (outcome, final_state, through[-1])


def per_device(
    skip_connection_stream,
    emitted_valve_unscaled,
    channel_source_mapped,
    hidden_source_mapped,
    probe_mapped_values,
    increment_premapped,
    extra_log_fading,
    channel_fading_speed,
    channel_source_kernel,
    hidden_source_kernel,
    probe_kernel_coefficients,
    cluster_scaling_factor,
    emitted_mapping_matrix,
    standardize_scaling,
    standardize_offset,
    chosen_specialist_ids,
    specialist_mixing_shares,
    specialist_gating_matrices,
    raising_matrices,
    lowering_matrices,
):
    sp_size = lax.axis_size("sp")
    sp_index = lax.axis_index("sp")
    tok_rows = skip_connection_stream.shape[1]
    model_width = skip_connection_stream.shape[2]
    inner_width = HEADS * HEAD_DIM
    per_group = HEADS // GROUPS
    paired = HEAD_DIM + 2 * STATE
    head_count = HEADS // sp_size
    first_head = sp_index * head_count
    x_heads = channel_source_mapped[0].reshape(tok_rows, HEADS, HEAD_DIM)
    b_heads = jnp.repeat(
        hidden_source_mapped[0].reshape(tok_rows, GROUPS, STATE), per_group, axis=1
    )
    c_heads = jnp.repeat(probe_mapped_values[0].reshape(tok_rows, GROUPS, STATE), per_group, axis=1)
    payload = jnp.concatenate([x_heads, b_heads, c_heads], axis=2)
    arrived = lax.all_to_all(payload, "sp", split_axis=1, concat_axis=0, tiled=True)
    taps_x = lax.dynamic_slice_in_dim(
        channel_source_kernel.reshape(KERNEL, HEADS, HEAD_DIM), first_head, head_count, 1
    )
    taps_b = lax.dynamic_slice_in_dim(
        jnp.repeat(hidden_source_kernel.reshape(KERNEL, GROUPS, STATE), per_group, axis=1),
        first_head,
        head_count,
        1,
    )
    taps_c = lax.dynamic_slice_in_dim(
        jnp.repeat(probe_kernel_coefficients.reshape(KERNEL, GROUPS, STATE), per_group, axis=1),
        first_head,
        head_count,
        1,
    )
    rim_rows = jnp.zeros((KERNEL - 1, head_count, paired), jnp.bfloat16)
    convolved = causal_conv(arrived, jnp.concatenate([taps_x, taps_b, taps_c], axis=2), rim_rows)
    increment_delta = jax.nn.softplus(increment_premapped[0])
    speeds_per_channel = lax.dynamic_slice_in_dim(channel_fading_speed, first_head, head_count, 0)
    fading_exponent = extra_log_fading[0] - speeds_per_channel[None, :] * increment_delta
    init_state = jnp.zeros((head_count, HEAD_DIM, STATE), jnp.float32)
    outcome, final_state, total_decay = ssd_blocks(
        convolved[:, :, :HEAD_DIM],
        convolved[:, :, HEAD_DIM : HEAD_DIM + STATE],
        convolved[:, :, HEAD_DIM + STATE :],
        increment_delta,
        fading_exponent,
        init_state,
        BLK,
    )
    returned_rows = lax.all_to_all(
        outcome.astype(jnp.bfloat16), "sp", split_axis=0, concat_axis=1, tiled=True
    )
    blending_outcome = returned_rows.reshape(tok_rows, inner_width)
    gated = blending_outcome.astype(jnp.float32) * jax.nn.silu(
        emitted_valve_unscaled[0].astype(jnp.float32)
    )
    grouped = gated.reshape(tok_rows, GROUPS, inner_width // GROUPS)
    grouped = grouped * lax.rsqrt(jnp.mean(grouped * grouped, axis=-1, keepdims=True) + rms_eps)
    group_normed = (
        grouped.reshape(tok_rows, inner_width) * cluster_scaling_factor[None, :]
    ).astype(jnp.bfloat16)
    pre_norm = skip_connection_stream[0].astype(jnp.float32) + jnp.dot(
        group_normed, emitted_mapping_matrix, preferred_element_type=jnp.float32
    )
    centre = jnp.mean(pre_norm, axis=-1, keepdims=True)
    variance = jnp.mean(jnp.square(pre_norm - centre), axis=-1, keepdims=True)
    normed = (
        (pre_norm - centre) * lax.rsqrt(variance + norm_eps) * standardize_scaling[None, :]
        + standardize_offset[None, :]
    ).astype(jnp.bfloat16)
    slot_cap = 3 * tok_rows // sp_size
    flat_ids = chosen_specialist_ids[0].reshape(-1)
    matched = (flat_ids[:, None] == jnp.arange(sp_size, dtype=jnp.int32)[None, :]).astype(jnp.int32)
    ranked = jnp.cumsum(matched, axis=0) - 1
    target = flat_ids * slot_cap + jnp.sum(matched * ranked, axis=1)
    placing = (jnp.arange(sp_size * slot_cap, dtype=jnp.int32)[:, None] == target[None, :]).astype(
        jnp.bfloat16
    )
    placing = jnp.sum(placing.reshape(sp_size * slot_cap, tok_rows, 2), axis=2)
    outgoing = (
        jnp.dot(placing, normed, preferred_element_type=jnp.float32)
        .astype(jnp.bfloat16)
        .reshape(sp_size, slot_cap, model_width)
    )
    arrived_rows = lax.all_gather(
        lax.all_to_all(outgoing, "sp", split_axis=0, concat_axis=0, tiled=True)[:, None],
        "dp",
        axis=1,
        tiled=True,
    )
    flattened = arrived_rows.reshape(-1, model_width)
    gate_val = jnp.dot(flattened, specialist_gating_matrices[0], preferred_element_type=jnp.float32)
    up_val = jnp.dot(flattened, raising_matrices[0], preferred_element_type=jnp.float32)
    hidden = (jax.nn.silu(gate_val) * up_val).astype(jnp.bfloat16)
    partial_value = jnp.dot(
        hidden, lowering_matrices[0], preferred_element_type=jnp.float32
    ).astype(jnp.bfloat16)
    partial_rows = (
        lax.optimization_barrier(partial_value).astype(jnp.float32).reshape(arrived_rows.shape)
    )
    summed = lax.psum_scatter(
        partial_rows.astype(jnp.bfloat16), "dp", scatter_dimension=1, tiled=True
    )
    item_count = partial_rows.shape[2]
    answer_rows = summed.reshape(sp_size, item_count, model_width)
    answered = lax.all_to_all(answer_rows, "sp", split_axis=0, concat_axis=0, tiled=True)
    picked = answered.reshape(sp_size * slot_cap, model_width)[target.reshape(tok_rows, 2)]
    routed_sum = jnp.sum(
        specialist_mixing_shares[0][:, :, None] * picked.astype(jnp.float32), axis=1
    )
    layer_out = (normed.astype(jnp.float32) + routed_sum).astype(jnp.bfloat16)
    return layer_out[None]


def solution(mesh):
    placed = (
        P("dp", "sp", None),
        P("dp", "sp", None),
        P("dp", "sp", None),
        P("dp", "sp", None),
        P("dp", "sp", None),
        P("dp", None, "sp"),
        P("dp", None, "sp"),
        P(),
        P(),
        P(),
        P(),
        P(),
        P(),
        P(),
        P(),
        P("dp", "sp", None),
        P("dp", "sp", None),
        P("sp", None, "dp"),
        P("sp", None, "dp"),
        P("sp", "dp", None),
    )
    return jax.shard_map(
        per_device, mesh=mesh, in_specs=placed, out_specs=P("dp", "sp", None), check_vma=False
    )
```

profile of v0, /device:TPU:0, one launch (start us, length us, event | category | flops | bytes accessed | tf_op | source)
XLA Modules:
  0.0 370.2 jit_solution(385357176187847751)
XLA Ops:
  6.6 1.0 copy.134
  7.6 1.0 copy.135
  8.6 1.1 copy.133
  9.8 0.9 pad_maximum_fusion
  10.7 7.3 %all-to-all-start = ((bf16[128,16,192]{0,2,1:T(8,128)(2,1)}), bf16[128,16,192]{0,2,1:T(8,128)(2,1)S(1)}, u32[]{:S(2)}, u32[]{:S(2)}) async-start(bf16[128,16,192]{0,2,1:T(8,128)(2,1)} %pad_maximum_fusion), calls=%async_computation | async-start | bytes 1572864 | tf_op jit(solution)/shard_map/all_to_all | solution.py:126
  21.2 17.0 %all-to-all-done = bf16[128,16,192]{0,2,1:T(8,128)(2,1)S(1)} async-done(((bf16[128,16,192]{0,2,1:T(8,128)(2,1)}), bf16[128,16,192]{0,2,1:T(8,128)(2,1)S(1)}, u32[]{:S(2)}, u32[]{:S(2)}) %all-to-all-start) | async-done | bytes 786464 | tf_op jit(solution)/shard_map/all_to_all | solution.py:126
  38.8 1.6 multiply_convert_fusion
  41.0 0.9 fusion.14
  43.6 1.1 reshape.249
  44.7 3.7 all-to-all-start.1
  48.8 8.7 %all-to-all-done.1 = bf16[8,2,8192]{2,1,0:T(2,128)(2,1)S(1)} async-done(((bf16[8,2,8192]{2,1,0:T(2,128)(2,1)}), bf16[8,2,8192]{2,1,0:T(2,128)(2,1)S(1)}, u32[]{:S(2)}, u32[]{:S(2)}) %all-to-all-start.1) | async-done | bytes 262176 | tf_op jit(solution)/shard_map/all_to_all | solution.py:157
  59.1 3.0 fusion.72
  63.1 40.2 %all_to_all.37 = bf16[8,48,2048]{2,1,0:T(8,128)(2,1)} all-to-all(bf16[8,48,2048]{2,1,0:T(8,128)(2,1)S(1)} %bitcast.198), channel_id=1, replica_groups=mesh['sp'=8,'dp'=4] {'sp'}, dimensions={0} | all-to-all | bytes 3145728 | tf_op jit(solution)/shard_map/all_to_all | solution.py:193
  103.5 45.2 %all-gather.3.cloned.1.call-done = bf16[8,192,2048]{2,1,0:T(8,128)(2,1)} async-done(((bf16[8,48,2048]{2,1,0:T(8,128)(2,1)}), bf16[8,192,2048]{2,1,0:T(8,128)(2,1)}) %all-gather.3.cloned.1.call-update) | async-done | bytes 6291472 | tf_op jit(solution)/shard_map/all_gather | solution.py:192
  148.8 13.8 %fusion.6 = f32[1536,1280]{1,0:T(8,128)} fusion(bf16[1536,2048]{1,0:T(8,128)(2,1)} %bitcast.220, bf16[1,2048,1280]{2,1,0:T(8,128)(2,1)} %param.37), kind=kOutput, calls=%fused_computation.7 | convolution fusion | flops 8053063680 | bytes 19398656 | tf_op jit(solution)/shard_map/dot_general | solution.py:199
  162.6 26.5 %fusion.2 = bf16[1536,2048]{1,0:T(8,128)(2,1)} fusion(bf16[1536,2048]{1,0:T(8,128)(2,1)} %bitcast.221, f32[1536,1280]{1,0:T(8,128)} %fusion.6, bf16[1,1280,2048]{2,1,0:T(8,128)(2,1)} %param.39, bf16[1,2048,1280]{2,1,0:T(8,128)(2,1)} %param.38), kind=kOutput, calls=%fused_computation.4 | convolution fusion | flops 16121069568 | bytes 30932992 | tf_op jit(solution)/shard_map/dot_general | solution.py:202
  190.4 118.5 %all-reduce.4.cloned.1.call-done = bf16[8,4,48,2048]{3,2,1,0:T(8,128)(2,1)} async-done(((bf16[8,4,48,2048]{3,2,1,0:T(8,128)(2,1)}), bf16[8,4,48,2048]{3,2,1,0:T(8,128)(2,1)}) %all-reduce.4.cloned.1.call-update) | async-done | bytes 6291472
  308.9 3.4 dynamic-slice_bitcast_fusion
  312.3 5.5 %all-to-all-start.3 = ((bf16[8,48,2048]{2,1,0:T(8,128)(2,1)}), bf16[8,48,2048]{2,1,0:T(8,128)(2,1)S(1)}, u32[]{:S(2)}, u32[]{:S(2)}) async-start(bf16[8,48,2048]{2,1,0:T(8,128)(2,1)} %dynamic-slice_bitcast_fusion), calls=%async_computation.3 | async-start | bytes 3145728 | tf_op jit(solution)/shard_map/all_to_all | solution.py:213
  318.2 36.2 %all-to-all-done.3 = bf16[8,48,2048]{2,1,0:T(8,128)(2,1)S(1)} async-done(((bf16[8,48,2048]{2,1,0:T(8,128)(2,1)}), bf16[8,48,2048]{2,1,0:T(8,128)(2,1)S(1)}, u32[]{:S(2)}, u32[]{:S(2)}) %all-to-all-start.3) | async-done | bytes 1572896 | tf_op jit(solution)/shard_map/all_to_all | solution.py:213
  354.4 2.3 gather_fusion
  356.8 2.4 reshape.242
  359.1 3.2 multiply_reduce_fusion
  362.3 1.1 fusion.21
  (102 shorter events, 10.7 us)
Async XLA Ops:
  6.5 11.5 %copy-start.13 = (f32[16]{0:T(128)S(1)}, f32[16]{0:T(128)}, u32[]{:S(2)}) copy-start(f32[16]{0:T(128)} %param.27) | copy-start | bytes 196
  6.5 11.6 %copy-start.4 = (f32[1,1024,2]{1,2,0:T(2,128)S(1)}, f32[1,1024,2]{1,2,0:T(2,128)}, u32[]{:S(2)}) copy-start(f32[1,1024,2]{1,2,0:T(2,128)} %param.25) | copy-start | bytes 24580
  6.5 11.6 %copy-start.6 = (f32[1,1024,2]{1,2,0:T(2,128)S(1)}, f32[1,1024,2]{1,2,0:T(2,128)}, u32[]{:S(2)}) copy-start(f32[1,1024,2]{1,2,0:T(2,128)} %param.26) | copy-start | bytes 24580
  6.5 12.7 %copy-start.11 = (s32[1,128,2]{1,2,0:T(2,128)S(1)}, s32[1,128,2]{1,2,0:T(2,128)}, u32[]{:S(2)}) copy-start(s32[1,128,2]{1,2,0:T(2,128)} %param.35) | copy-start | bytes 3076
  6.5 13.1 %copy-start.9 = (f32[4,256]{1,0:T(4,128)S(1)}, f32[4,256]{1,0:T(4,128)}, u32[]{:S(2)}) copy-start(f32[4,256]{1,0:T(4,128)} %param.29) | copy-start | bytes 12292
  6.5 13.2 %copy-start.10 = (f32[4,256]{1,0:T(4,128)S(1)}, f32[4,256]{1,0:T(4,128)}, u32[]{:S(2)}) copy-start(f32[4,256]{1,0:T(4,128)} %param.30) | copy-start | bytes 12292
  6.6 13.2 %copy-start.5 = (f32[4,1024]{1,0:T(4,128)S(1)}, f32[4,1024]{1,0:T(4,128)}, u32[]{:S(2)}) copy-start(f32[4,1024]{1,0:T(4,128)} %param.28) | copy-start | bytes 49156
  6.6 13.3 %copy-start.1 = (bf16[1,128,1024]{2,1,0:T(8,128)(2,1)S(1)}, bf16[1,128,1024]{2,1,0:T(8,128)(2,1)}, u32[]{:S(2)}) copy-start(bf16[1,128,1024]{2,1,0:T(8,128)(2,1)} %param.21) | copy-start | bytes 786436
  10.7 27.5 %all-to-all-start = ((bf16[128,16,192]{0,2,1:T(8,128)(2,1)}), bf16[128,16,192]{0,2,1:T(8,128)(2,1)S(1)}, u32[]{:S(2)}, u32[]{:S(2)}) async-start(bf16[128,16,192]{0,2,1:T(8,128)(2,1)} %pad_maximum_fusion), calls=%async_computation | async-start | bytes 1572864 | tf_op jit(solution)/shard_map/all_to_all | solution.py:126
  21.0 19.4 %copy-start.7 = (s32[8,3]{0,1:T(4,128)}, s32[8,3]{0,1:T(4,128)S(1)}, u32[]{:S(2)}) copy-start(s32[8,3]{0,1:T(4,128)S(1)} %reduce-window.9) | copy-start | bytes 292
  41.0 7.4 %slice-start = ((s32[8,3]{0,1:T(4,128)}), s32[8,2]{0,1:T(2,128)S(1)}, s32[]{:S(2)}) async-start(s32[8,3]{0,1:T(4,128)} %copy-done.7), calls=%async_computation.6 | async-start | bytes 2048 | tf_op jit(solution)/shard_map/slice.1
  43.1 15.7 %copy-start.8 = (f32[1024]{0:T(1024)S(1)}, f32[1024]{0:T(1024)}, u32[]{:S(2)}) copy-start(f32[1024]{0:T(1024)} %param.31) | copy-start | bytes 12292
  44.7 14.5 %copy-start = (bf16[1,128,2048]{2,1,0:T(8,128)(2,1)S(1)}, bf16[1,128,2048]{2,1,0:T(8,128)(2,1)}, u32[]{:S(2)}) copy-start(bf16[1,128,2048]{2,1,0:T(8,128)(2,1)} %param.20) | copy-start | bytes 1572868
  44.7 12.8 %all-to-all-start.1 = ((bf16[8,2,8192]{2,1,0:T(2,128)(2,1)}), bf16[8,2,8192]{2,1,0:T(2,128)(2,1)S(1)}, u32[]{:S(2)}, u32[]{:S(2)}) async-start(bf16[8,2,8192]{2,1,0:T(2,128)(2,1)} %reshape.249), calls=%async_computation.1 | async-start | bytes 524288 | tf_op jit(solution)/shard_map/all_to_all | solution.py:157
  48.4 100.4 %all-gather.3.cloned.1.call-start = ((), (), s32[]{:S(2)}) async-start(), calls=%async_computation.4 | async-start | bytes 7864320 | tf_op jit(solution)/shard_map/all_gather | solution.py:192
  58.9 3.5 copy-start.2
  58.9 3.5 copy-start.3
  103.3 205.6 %all-reduce.4.cloned.1.call-start = ((), (), s32[]{:S(2)}) async-start(), calls=%async_computation.5 | async-start | bytes 12582912
  189.1 0.7 copy-start.14
  189.2 128.9 %copy-start.12 = (f32[1,128,2]{1,2,0:T(2,128)S(1)}, f32[1,128,2]{1,2,0:T(2,128)}, u32[]{:S(2)}) copy-start(f32[1,128,2]{1,2,0:T(2,128)} %param.36) | copy-start | bytes 3076
  312.3 42.1 %all-to-all-start.3 = ((bf16[8,48,2048]{2,1,0:T(8,128)(2,1)}), bf16[8,48,2048]{2,1,0:T(8,128)(2,1)S(1)}, u32[]{:S(2)}, u32[]{:S(2)}) async-start(bf16[8,48,2048]{2,1,0:T(8,128)(2,1)} %dynamic-slice_bitcast_fusion), calls=%async_computation.3 | async-start | bytes 3145728 | tf_op jit(solution)/shard_map/all_to_all | solution.py:213
Sparse Core Ops, SparseCore 0:
  103.4 45.3 all-gather.2
  189.3 119.5 all-reduce.3
where the time goes:
time: 371 us; the launch traced here: 370 us
  waiting for transfers between devices  226 us (61%)
  matrix products  46.4 us (13%)
  blocking collectives  40.2 us (11%)
  local copies, waits for them, and re-layouts  17.3 us (5%)
  starting transfers between devices  16.8 us (5%)
  between operations  13.9 us (4%)
  other arithmetic  9.97 us (3%)
    unnamed x3, waiting for transfers between devices  119 us
    all_gather x1, waiting for transfers between devices, per_device(): lax.all_gather(lax.all_to_all(outgoing, 'sp', split_axis=0, concat_axis=0...  45.2 us
    all_to_all x1, blocking collectives, per_device(): lax.all_to_all(outgoing, 'sp', split_axis=0, concat_axis=0, tiled=True)  40.2 us
    all_to_all x1, waiting for transfers between devices, per_device(): lax.all_to_all(answer_rows, 'sp', split_axis=0, concat_axis=0, tiled=True)  36.2 us
    dot_general x1, matrix products, per_device(): jnp.dot(hidden, lowering_matrices[0], preferred_element_type=jnp.float32)  26.5 us
    all_to_all x1, waiting for transfers between devices, per_device(): lax.all_to_all(payload, 'sp', split_axis=1, concat_axis=0, tiled=True)  17 us
    dot_general x1, matrix products, per_device(): jnp.dot(flattened, specialist_gating_matrices[0], preferred_element_type=...  13.8 us
    all_to_all x1, waiting for transfers between devices, per_device(): lax.all_to_all(outcome.astype(jnp.bfloat16), 'sp', split_axis=0, concat_a...  8.66 us
  transfers between devices with their start and end apart: 5, of which 5 were waited for; matrix products, arithmetic and copies ran while one was open for 1% of the time, Pallas kernels for 0%

commit v1 on v0

--- a/solution.py
+++ b/solution.py
@@ -1,6 +1,10 @@
+import functools
+
 import jax
 import jax.numpy as jnp
 from jax import lax
+from jax.experimental import pallas as pl
+from jax.experimental.pallas import tpu as pltpu
 from jax.sharding import PartitionSpec as P
 
 HEADS = 16
@@ -84,6 +88,235 @@
         + jnp.exp(through[-1])[:, None, None] * init_state
     )
     return (outcome, final_state, through[-1])
+
+MESH = pl.DeviceIdType.MESH
+
+
+def flip(value, mask):
+    result, bit = value, 1
+    while bit <= mask:
+        if mask & bit:
+            result = result + bit * (1 - 2 * ((value // bit) % 2))
+        bit *= 2
+    return result
+
+
+def expert_kernel(
+    S, R, cap, group, out_ref, wg_hbm, wu_hbm, wd_hbm, ret_ref,
+    arr, hid, ra, rx, sx, fin, wg, wu, wd,
+    wsem, own_sem, d_s, d_r, g_s, g_r, a_s, a_r, x_s, x_r, b_s, b_r,
+):
+    s = lax.axis_index("sp")
+    d = lax.axis_index("dp")
+    nx = R // 2
+    steps = S // group
+    order = [0] + list(range(steps - 1, 0, -1))
+    members = [[p * group + i for i in range(group)] for p in order]
+    width = wd.shape[1]
+    ff = wg.shape[1]
+    f32 = jnp.float32
+
+    def rows(j, dc, dx, count=1):
+        return pl.ds((j * R + dc * nx + dx) * cap, count * cap)
+
+    def remote(src, dst, send, recv, where):
+        return pltpu.make_async_remote_copy(
+            src_ref=src, dst_ref=dst, send_sem=send, recv_sem=recv,
+            device_id=where, device_id_type=MESH,
+        )
+
+    def disp(j):
+        return remote(out_ref.at[pl.ds(j * cap, cap)], arr.at[rows(j, 0, 0)],
+                      d_s.at[j], d_r.at[j], {"sp": flip(s, j)})
+
+    def agx(j, dx):
+        return remote(arr.at[rows(j, 0, 0)], arr.at[rows(j, 0, dx)],
+                      g_s.at[j, dx], g_r.at[j, dx], {"dp": flip(d, 2 * dx)})
+
+    def agc(j, dx):
+        return remote(arr.at[rows(j, 0, dx)], arr.at[rows(j, 1, dx)],
+                      g_s.at[j, nx + dx], g_r.at[j, nx + dx], {"dp": flip(d, 1)})
+
+    def rsc(j):
+        return remote(arr.at[rows(j, 1, 0, nx)], ra.at[pl.ds(j * nx * cap, nx * cap)],
+                      a_s.at[j], a_r.at[j], {"dp": flip(d, 1)})
+
+    def rsx(j, dx):
+        at = pl.ds((j * (nx - 1) + dx - 1) * cap, cap)
+        return remote(sx.at[at], rx.at[at], x_s.at[j, dx], x_r.at[j, dx], {"dp": flip(d, 2 * dx)})
+
+    def back(j):
+        return remote(fin.at[pl.ds(j * cap, cap)], ret_ref.at[pl.ds(j * cap, cap)],
+                      b_s.at[j], b_r.at[j], {"sp": flip(s, j)})
+
+    own = pltpu.make_async_copy(out_ref.at[pl.ds(0, cap)], arr.at[rows(0, 0, 0)], own_sem)
+    loads = [
+        pltpu.make_async_copy(src, dst, wsem.at[i])
+        for i, (src, dst) in enumerate(((wg_hbm, wg), (wu_hbm, wu), (wd_hbm, wd)))
+    ]
+    own.start()
+    for load in loads:
+        load.start()
+
+    barrier = pltpu.get_barrier_semaphore()
+    peers = [{"sp": flip(s, j)} for j in range(1, S)]
+    peers += [{"dp": flip(d, 1)}] + [{"dp": flip(d, 2 * dx)} for dx in range(1, nx)]
+    for peer in peers:
+        pl.semaphore_signal(barrier, inc=1, device_id=peer, device_id_type=MESH)
+    pl.semaphore_wait(barrier, len(peers))
+
+    for js in members:
+        for j in js:
+            if j:
+                disp(j).start()
+
+    def arrive(p):
+        for j in members[p]:
+            if j:
+                disp(j).wait_recv()
+            else:
+                own.wait()
+            for dx in range(1, nx):
+                agx(j, dx).start()
+            agc(j, 0).start()
+
+    def relay(p):
+        for j in members[p]:
+            for dx in range(1, nx):
+                agx(j, dx).wait_recv()
+                agc(j, dx).start()
+
+    def span(p):
+        return pl.ds(order[p] * group * R * cap, group * R * cap)
+
+    def gate_up(p):
+        for j in members[p]:
+            for dx in range(nx):
+                agc(j, dx).wait_recv()
+        wide = 256 if ff % 256 == 0 else 128
+
+        def piece(i, carry):
+            cols = pl.ds(pl.multiple_of(i * wide, wide), wide)
+            x = arr[span(p), :]
+            g = jnp.dot(x, wg[:, cols], preferred_element_type=f32)
+            u = jnp.dot(x, wu[:, cols], preferred_element_type=f32)
+            hid[:, cols] = (jax.nn.silu(g) * u).astype(jnp.bfloat16)
+            return carry
+
+        lax.fori_loop(0, ff // wide, piece, 0)
+
+    def down(p):
+        for j in members[p]:
+            for dx in range(nx):
+                if dx:
+                    agx(j, dx).wait_send()
+                agc(j, dx).wait_send()
+        wide = 256 if width % 256 == 0 else 128
+
+        def piece(i, carry):
+            cols = pl.ds(pl.multiple_of(i * wide, wide), wide)
+            arr[span(p), cols] = jnp.dot(
+                hid[...], wd[:, cols], preferred_element_type=f32
+            ).astype(jnp.bfloat16)
+            return carry
+
+        lax.fori_loop(0, width // wide, piece, 0)
+        for j in members[p]:
+            rsc(j).start()
+
+    def chip_sum(p):
+        for j in members[p]:
+            rsc(j).wait_recv()
+            for dx in range(1, nx):
+                both = (
+                    arr[rows(j, 0, dx), :].astype(f32)
+                    + ra[pl.ds((j * nx + dx) * cap, cap), :].astype(f32)
+                )
+                sx[pl.ds((j * (nx - 1) + dx - 1) * cap, cap), :] = both.astype(jnp.bfloat16)
+                rsx(j, dx).start()
+
+    def finish(p):
+        for j in members[p]:
+            total = (
+                arr[rows(j, 0, 0), :].astype(f32)
+                + ra[pl.ds(j * nx * cap, cap), :].astype(f32)
+            )
+            for dx in range(1, nx):
+                rsx(j, dx).wait_recv()
+                total = total + rx[pl.ds((j * (nx - 1) + dx - 1) * cap, cap), :].astype(f32)
+            if j:
+                fin[pl.ds(j * cap, cap), :] = total.astype(jnp.bfloat16)
+                back(j).start()
+            else:
+                ret_ref[pl.ds(0, cap), :] = total.astype(jnp.bfloat16)
+
+    arrive(0)
+    loads[0].wait()
+    loads[1].wait()
+    for p in range(steps):
+        relay(p)
+        gate_up(p)
+        if p + 1 < steps:
+            arrive(p + 1)
+        if p == 0:
+            loads[2].wait()
+        if p > 1:
+            finish(p - 2)
+        if p:
+            chip_sum(p - 1)
+        down(p)
+    if steps > 1:
+        finish(steps - 2)
+    chip_sum(steps - 1)
+    finish(steps - 1)
+
+    for j in range(S):
+        rsc(j).wait_send()
+        for dx in range(1, nx):
+            rsx(j, dx).wait_send()
+        if j:
+            disp(j).wait_send()
+            back(j).wait_send()
+            back(j).wait_recv()
+
+
+def run_experts(outgoing, gate_w, up_w, down_w, S, R, cap):
+    width, ff = gate_w.shape
+    nx = R // 2
+    group = 2
+    bf = jnp.bfloat16
+    dma = pltpu.SemaphoreType.DMA
+    total = S * R * cap
+    return pl.pallas_call(
+        functools.partial(expert_kernel, S, R, cap, group),
+        out_shape=jax.ShapeDtypeStruct((S * cap, width), bf),
+        in_specs=[pl.BlockSpec(memory_space=pltpu.VMEM)]
+        + [pl.BlockSpec(memory_space=pl.ANY)] * 3,
+        out_specs=pl.BlockSpec(memory_space=pltpu.VMEM),
+        scratch_shapes=[
+            pltpu.VMEM((total, width), bf),
+            pltpu.VMEM((group * R * cap, ff), bf),
+            pltpu.VMEM((S * nx * cap, width), bf),
+            pltpu.VMEM((S * (nx - 1) * cap, width), bf),
+            pltpu.VMEM((S * (nx - 1) * cap, width), bf),
+            pltpu.VMEM((S * cap, width), bf),
+            pltpu.VMEM((width, ff), bf),
+            pltpu.VMEM((width, ff), bf),
+            pltpu.VMEM((ff, width), bf),
+            dma((3,)), dma(()),
+            dma((S,)), dma((S,)),
+            dma((S, R)), dma((S, R)),
+            dma((S,)), dma((S,)),
+            dma((S, nx)), dma((S, nx)),
+            dma((S,)), dma((S,)),
+        ],
+        compiler_params=pltpu.CompilerParams(
+            collective_id=0, has_side_effects=True, vmem_limit_bytes=58 * 1024 * 1024
+        ),
+        cost_estimate=pl.CostEstimate(
+            flops=6 * total * width * ff, bytes_accessed=6 * width * ff, transcendentals=total * ff
+        ),
+    )(outgoing, gate_w, up_w, down_w)
 
 
 def per_device(
@@ -114,41 +347,49 @@
     model_width = skip_connection_stream.shape[2]
     inner_width = HEADS * HEAD_DIM
     per_group = HEADS // GROUPS
-    paired = HEAD_DIM + 2 * STATE
     head_count = HEADS // sp_size
     first_head = sp_index * head_count
-    x_heads = channel_source_mapped[0].reshape(tok_rows, HEADS, HEAD_DIM)
-    b_heads = jnp.repeat(
-        hidden_source_mapped[0].reshape(tok_rows, GROUPS, STATE), per_group, axis=1
-    )
-    c_heads = jnp.repeat(probe_mapped_values[0].reshape(tok_rows, GROUPS, STATE), per_group, axis=1)
-    payload = jnp.concatenate([x_heads, b_heads, c_heads], axis=2)
-    arrived = lax.all_to_all(payload, "sp", split_axis=1, concat_axis=0, tiled=True)
-    taps_x = lax.dynamic_slice_in_dim(
-        channel_source_kernel.reshape(KERNEL, HEADS, HEAD_DIM), first_head, head_count, 1
-    )
-    taps_b = lax.dynamic_slice_in_dim(
-        jnp.repeat(hidden_source_kernel.reshape(KERNEL, GROUPS, STATE), per_group, axis=1),
-        first_head,
-        head_count,
-        1,
-    )
-    taps_c = lax.dynamic_slice_in_dim(
-        jnp.repeat(probe_kernel_coefficients.reshape(KERNEL, GROUPS, STATE), per_group, axis=1),
-        first_head,
-        head_count,
-        1,
-    )
-    rim_rows = jnp.zeros((KERNEL - 1, head_count, paired), jnp.bfloat16)
-    convolved = causal_conv(arrived, jnp.concatenate([taps_x, taps_b, taps_c], axis=2), rim_rows)
+    span = max(1, head_count // per_group)
+    copies = max(1, per_group // head_count)
+    x_part = channel_source_mapped[0].reshape(tok_rows, sp_size, head_count * HEAD_DIM)
+    b_part = hidden_source_mapped[0].reshape(tok_rows, GROUPS // span, span * STATE)
+    c_part = probe_mapped_values[0].reshape(tok_rows, GROUPS // span, span * STATE)
+    payload = jnp.concatenate(
+        [x_part, jnp.repeat(b_part, copies, axis=1), jnp.repeat(c_part, copies, axis=1)], axis=2
+    )
+    sent_width = payload.shape[2]
+    arrived = lax.all_to_all(
+        payload.reshape(tok_rows, sp_size * sent_width), "sp", split_axis=1, concat_axis=0, tiled=True
+    )
+    x_width, s_width = head_count * HEAD_DIM, span * STATE
+    state_at = (sp_index // copies) * s_width
+    taps = jnp.concatenate(
+        [
+            lax.dynamic_slice_in_dim(channel_source_kernel, sp_index * x_width, x_width, 1),
+            lax.dynamic_slice_in_dim(hidden_source_kernel, state_at, s_width, 1),
+            lax.dynamic_slice_in_dim(probe_kernel_coefficients, state_at, s_width, 1),
+        ],
+        axis=1,
+    )
+    rim_rows = jnp.zeros((KERNEL - 1, sent_width), jnp.bfloat16)
+    flat_conv = causal_conv(arrived, taps, rim_rows)
+    seq_rows = flat_conv.shape[0]
+    x_conv = flat_conv[:, :x_width].reshape(seq_rows, head_count, HEAD_DIM)
+    shared = head_count // span
+    b_conv = jnp.repeat(
+        flat_conv[:, x_width : x_width + s_width].reshape(seq_rows, span, STATE), shared, axis=1
+    )
+    c_conv = jnp.repeat(
+        flat_conv[:, x_width + s_width :].reshape(seq_rows, span, STATE), shared, axis=1
+    )
     increment_delta = jax.nn.softplus(increment_premapped[0])
     speeds_per_channel = lax.dynamic_slice_in_dim(channel_fading_speed, first_head, head_count, 0)
     fading_exponent = extra_log_fading[0] - speeds_per_channel[None, :] * increment_delta
     init_state = jnp.zeros((head_count, HEAD_DIM, STATE), jnp.float32)
     outcome, final_state, total_decay = ssd_blocks(
-        convolved[:, :, :HEAD_DIM],
-        convolved[:, :, HEAD_DIM : HEAD_DIM + STATE],
-        convolved[:, :, HEAD_DIM + STATE :],
+        x_conv,
+        b_conv,
+        c_conv,
         increment_delta,
         fading_exponent,
         init_state,
@@ -175,46 +416,33 @@
         (pre_norm - centre) * lax.rsqrt(variance + norm_eps) * standardize_scaling[None, :]
         + standardize_offset[None, :]
     ).astype(jnp.bfloat16)
-    slot_cap = 3 * tok_rows // sp_size
+    slot_cap = -(-(3 * tok_rows // sp_size) // 16) * 16
+    dp_size = lax.axis_size("dp")
+    slots = sp_size * slot_cap
     flat_ids = chosen_specialist_ids[0].reshape(-1)
     matched = (flat_ids[:, None] == jnp.arange(sp_size, dtype=jnp.int32)[None, :]).astype(jnp.int32)
     ranked = jnp.cumsum(matched, axis=0) - 1
-    target = flat_ids * slot_cap + jnp.sum(matched * ranked, axis=1)
-    placing = (jnp.arange(sp_size * slot_cap, dtype=jnp.int32)[:, None] == target[None, :]).astype(
-        jnp.bfloat16
-    )
-    placing = jnp.sum(placing.reshape(sp_size * slot_cap, tok_rows, 2), axis=2)
-    outgoing = (
-        jnp.dot(placing, normed, preferred_element_type=jnp.float32)
-        .astype(jnp.bfloat16)
-        .reshape(sp_size, slot_cap, model_width)
-    )
-    arrived_rows = lax.all_gather(
-        lax.all_to_all(outgoing, "sp", split_axis=0, concat_axis=0, tiled=True)[:, None],
-        "dp",
-        axis=1,
-        tiled=True,
-    )
-    flattened = arrived_rows.reshape(-1, model_width)
-    gate_val = jnp.dot(flattened, specialist_gating_matrices[0], preferred_element_type=jnp.float32)
-    up_val = jnp.dot(flattened, raising_matrices[0], preferred_element_type=jnp.float32)
-    hidden = (jax.nn.silu(gate_val) * up_val).astype(jnp.bfloat16)
-    partial_value = jnp.dot(
-        hidden, lowering_matrices[0], preferred_element_type=jnp.float32
-    ).astype(jnp.bfloat16)
-    partial_rows = (
-        lax.optimization_barrier(partial_value).astype(jnp.float32).reshape(arrived_rows.shape)
-    )
-    summed = lax.psum_scatter(
-        partial_rows.astype(jnp.bfloat16), "dp", scatter_dimension=1, tiled=True
-    )
-    item_count = partial_rows.shape[2]
-    answer_rows = summed.reshape(sp_size, item_count, model_width)
-    answered = lax.all_to_all(answer_rows, "sp", split_axis=0, concat_axis=0, tiled=True)
-    picked = answered.reshape(sp_size * slot_cap, model_width)[target.reshape(tok_rows, 2)]
-    routed_sum = jnp.sum(
-        specialist_mixing_shares[0][:, :, None] * picked.astype(jnp.float32), axis=1
-    )
+    relative = jnp.bitwise_xor(flat_ids, sp_index)
+    target = (relative * slot_cap + jnp.sum(matched * ranked, axis=1)).reshape(tok_rows, 2)
+    placing = jnp.arange(slots, dtype=jnp.int32)[:, None]
+    placing = ((placing == target[None, :, 0]) | (placing == target[None, :, 1])).astype(jnp.bfloat16)
+    outgoing = jnp.dot(placing, normed, preferred_element_type=jnp.float32).astype(jnp.bfloat16)
+    answered = run_experts(
+        outgoing,
+        specialist_gating_matrices[0],
+        raising_matrices[0],
+        lowering_matrices[0],
+        sp_size,
+        dp_size,
+        slot_cap,
+    )
+    slot_index = jnp.arange(slots, dtype=jnp.int32)[None, :]
+    routed_sum = jnp.zeros((tok_rows, model_width), jnp.float32)
+    for choice in range(2):
+        picking = (slot_index == target[:, choice : choice + 1]).astype(jnp.bfloat16)
+        routed_sum = routed_sum + specialist_mixing_shares[0][:, choice : choice + 1] * jnp.dot(
+            picking, answered, preferred_element_type=jnp.float32
+        )
     layer_out = (normed.astype(jnp.float32) + routed_sum).astype(jnp.bfloat16)
     return layer_out[None]
 

time: 371 us -> 170 us (0.46)
  waiting for transfers between devices: 226 us -> 20.3 us
  Pallas kernels: 0 us -> 115 us
  blocking collectives: 40.2 us -> 0 us
  matrix products: 46.4 us -> 10.7 us
  between operations: 13.9 us -> 0.45 us
  local copies, waits for them, and re-layouts: 17.3 us -> 8.1 us
  starting transfers between devices: 16.8 us -> 10.9 us
  other arithmetic: 9.97 us -> 4.3 us
    unnamed x3 -> x0, waiting for transfers between devices: 119 us -> none
    pallas_call x0 -> x1, Pallas kernels: none -> 115 us  [run_experts(): pl.pallas_call(functools.partial(expert_kernel, S, R, cap, group), out_sh...]
    all_gather x1 -> x0, waiting for transfers between devices: 45.2 us -> none  [per_device(): lax.all_gather(lax.all_to_all(outgoing, 'sp', split_axis=0, concat_axis=0...]
    all_to_all x2 -> x1, waiting for transfers between devices: 53.2 us -> 11.5 us  [per_device(): lax.all_to_all(payload.reshape(tok_rows, sp_size * sent_width), 'sp', spl...]
    all_to_all x1 -> x0, blocking collectives: 40.2 us -> none  [per_device(): lax.all_to_all(outgoing, 'sp', split_axis=0, concat_axis=0, tiled=True)]
    dot_general x2, matrix products: 40.4 us -> 3.41 us  [per_device(): jnp.dot(picking, answered, preferred_element_type=jnp.float32)]
    all_to_all x2 -> x1, starting transfers between devices: 12.8 us -> 7.31 us  [per_device(): lax.all_to_all(payload.reshape(tok_rows, sp_size * sent_width), 'sp', spl...]
  transfers between devices with their start and end apart: 5 -> 2, of which waited for: 5 -> 2; matrix products, arithmetic and copies ran while one was open for 1% -> 2% of each run, Pallas kernels for 0% -> 0%
where the time goes in v1:
time: 170 us
  Pallas kernels  115 us (68%)
  waiting for transfers between devices  20.3 us (12%)
  starting transfers between devices  10.9 us (6%)
  matrix products  10.7 us (6%)
  local copies, waits for them, and re-layouts  8.1 us (5%)
  other arithmetic  4.3 us (3%)
    pallas_call x1, Pallas kernels, run_experts(): pl.pallas_call(functools.partial(expert_kernel, S, R, cap, group), out_sh...  115 us
    all_to_all x1, waiting for transfers between devices, per_device(): lax.all_to_all(payload.reshape(tok_rows, sp_size * sent_width), 'sp', spl...  11.5 us
    all_to_all x1, waiting for transfers between devices, per_device(): lax.all_to_all(outcome.astype(jnp.bfloat16), 'sp', split_axis=0, concat_a...  8.82 us
    all_to_all x1, starting transfers between devices, per_device(): lax.all_to_all(payload.reshape(tok_rows, sp_size * sent_width), 'sp', spl...  7.31 us
    unnamed x37, local copies, waits for them, and re-layouts  5.33 us
    all_to_all x1, starting transfers between devices, per_device(): lax.all_to_all(outcome.astype(jnp.bfloat16), 'sp', split_axis=0, concat_a...  3.64 us
    dot_general x2, matrix products, per_device(): jnp.dot(picking, answered, preferred_element_type=jnp.float32)  3.41 us
  transfers between devices with their start and end apart: 2, of which 2 were waited for; matrix products, arithmetic and copies ran while one was open for 2% of the time, Pallas kernels for 0%

profile of v1, /device:TPU:0, one launch (start us, length us, event | category | flops | bytes accessed | tf_op | source)
XLA Modules:
  0.0 169.5 jit_solution(6202848231426594817)
XLA Ops:
  0.0 1.2 copy.102
  1.2 1.0 copy.103
  2.2 1.0 copy.104
  3.2 0.8 pad_maximum_fusion
  4.0 7.3 %all-to-all-start = ((bf16[128,8,256]{0,2,1:T(8,128)(2,1)}), bf16[128,8,256]{0,2,1:T(8,128)(2,1)S(1)}, u32[]{:S(2)}, u32[]{:S(2)}) async-start(bf16[128,8,256]{0,2,1:T(8,128)(2,1)} %pad_maximum_fusion), calls=%async_computation | async-start | bytes 1048576 | tf_op jit(solution)/shard_map/all_to_all | solution.py:361
  11.5 0.6 reduce_window_sum.35
  12.7 0.6 reduce-window.6
  14.3 11.5 %all-to-all-done = bf16[128,8,256]{0,2,1:T(8,128)(2,1)S(1)} async-done(((bf16[128,8,256]{0,2,1:T(8,128)(2,1)}), bf16[128,8,256]{0,2,1:T(8,128)(2,1)S(1)}, u32[]{:S(2)}, u32[]{:S(2)}) %all-to-all-start) | async-done | bytes 524320 | tf_op jit(solution)/shard_map/all_to_all | solution.py:361
  26.2 0.6 multiply_convert_fusion
  27.8 0.9 fusion.6
  28.7 0.4 fusion.8
  29.1 0.8 fusion.9
  29.9 0.4 copy.131
  30.4 1.1 reshape.147
  31.4 3.6 %all-to-all-start.1 = ((bf16[8,2,8192]{2,1,0:T(2,128)(2,1)}), bf16[8,2,8192]{2,1,0:T(2,128)(2,1)S(1)}, u32[]{:S(2)}, u32[]{:S(2)}) async-start(bf16[8,2,8192]{2,1,0:T(2,128)(2,1)} %reshape.147), calls=%async_computation.1 | async-start | bytes 524288 | tf_op jit(solution)/shard_map/all_to_all | solution.py:398
  35.4 8.8 %all-to-all-done.1 = bf16[8,2,8192]{2,1,0:T(2,128)(2,1)S(1)} async-done(((bf16[8,2,8192]{2,1,0:T(2,128)(2,1)}), bf16[8,2,8192]{2,1,0:T(2,128)(2,1)S(1)}, u32[]{:S(2)}, u32[]{:S(2)}) %all-to-all-start.1) | async-done | bytes 262176 | tf_op jit(solution)/shard_map/all_to_all | solution.py:398
  44.2 0.3 reshape.148
  44.5 0.4 copy.120
  45.1 0.4 multiply_reduce_fusion.1
  46.1 3.0 %fusion.64 = (f32[128]{0:T(128)S(1)}, f32[128,2048]{1,0:T(8,128)S(1)}) fusion(bf16[128,1024]{0,1:T(8,128)(2,1)S(1)} %fusion.17, bf16[1024,2048]{1,0:T(8,128)(2,1)} %param.32, bf16[1,128,2048]{2,1,0:T(8,128)(2,1)S(1)} %copy-done.2), kind=kOutput, calls=%fused_computation.113 | convolution fusion | flops 537657216 | bytes 6029824 | tf_op jit(solution)/shard_map/dot_general | solution.py:410
  49.5 1.8 %convolution_convert_fusion.out_ref = bf16[384,2048]{1,0:T(8,128)(2,1)} fusion(s32[128]{0:T(128)S(1)} %get-tuple-element.18, s32[128]{0:T(128)S(1)} %get-tuple-element.17, f32[128,2048]{1,0:T(8,128)S(1)} %get-tuple-element.20, f32[2048]{0:T(1024)S(1)} %copy-done.4, f32[2048]{0:T(1024)S(1)} %copy-done.5, f32[128]{0:T(128)S(1)} %add_rsqrt_fusion.1, ...), kind=kOutput, calls=%fused_computation | convolution fusion | flops 203571200 | bytes 2639872 | tf_op jit(solution)/shard_map/dot_general | solution.py:429
  51.3 114.8 %shard_map.190 = bf16[384,2048]{1,0:T(8,128)(2,1)} custom-call(bf16[384,2048]{1,0:T(8,128)(2,1)} %convolution_convert_fusion.out_ref, bf16[2048,1280]{1,0:T(8,128)(2,1)} %bitcast.172, bf16[2048,1280]{1,0:T(8,128)(2,1)} %bitcast.173, bf16[1280,2048]{1,0:T(8,128)(2,1)} %bitcast.174), custom_call_target="tpu_custom_call" | custom-call | flops 24159191040 | bytes 15728640 | tf_op jit(solution)/shard_map/pallas_call | solution.py:290
  166.1 2.0 %convolution_multiply_fusion.1 = f32[128,2048]{1,0:T(8,128)S(1)} fusion(bf16[384,2048]{1,0:T(8,128)(2,1)} %shard_map.190, f32[128]{0:T(128)S(1)} %get-tuple-element.16, s32[128]{0:T(128)S(1)} %get-tuple-element.17), kind=kOutput, calls=%fused_computation.4 | convolution fusion | flops 201637888 | bytes 2622464 | tf_op jit(solution)/shard_map/dot_general | solution.py:443
  168.1 1.4 fusion.3
  (80 shorter events, 4.4 us)
Async XLA Ops:
  0.0 14.1 %copy-start = (f32[4,1024]{1,0:T(4,128)S(1)}, f32[4,1024]{1,0:T(4,128)}, u32[]{:S(2)}) copy-start(f32[4,1024]{1,0:T(4,128)} %param.28) | copy-start | bytes 49156
  0.0 11.3 %copy-start.13 = (f32[16]{0:T(128)S(1)}, f32[16]{0:T(128)}, u32[]{:S(2)}) copy-start(f32[16]{0:T(128)} %param.27) | copy-start | bytes 196
  0.0 11.4 %copy-start.6 = (f32[1,1024,2]{1,2,0:T(2,128)S(1)}, f32[1,1024,2]{1,2,0:T(2,128)}, u32[]{:S(2)}) copy-start(f32[1,1024,2]{1,2,0:T(2,128)} %param.25) | copy-start | bytes 24580
  0.0 11.4 %copy-start.7 = (f32[1,1024,2]{1,2,0:T(2,128)S(1)}, f32[1,1024,2]{1,2,0:T(2,128)}, u32[]{:S(2)}) copy-start(f32[1,1024,2]{1,2,0:T(2,128)} %param.26) | copy-start | bytes 24580
  0.0 12.2 %copy-start.9 = (s32[1,128,2]{1,2,0:T(2,128)S(1)}, s32[1,128,2]{1,2,0:T(2,128)}, u32[]{:S(2)}) copy-start(s32[1,128,2]{1,2,0:T(2,128)} %param.35) | copy-start | bytes 3076
  3.1 11.0 %copy-start.10 = (f32[4,256]{1,0:T(4,128)S(1)}, f32[4,256]{1,0:T(4,128)}, u32[]{:S(2)}) copy-start(f32[4,256]{1,0:T(4,128)} %param.30) | copy-start | bytes 12292
  3.1 11.0 %copy-start.11 = (f32[4,256]{1,0:T(4,128)S(1)}, f32[4,256]{1,0:T(4,128)}, u32[]{:S(2)}) copy-start(f32[4,256]{1,0:T(4,128)} %param.29) | copy-start | bytes 12292
  4.0 21.8 %all-to-all-start = ((bf16[128,8,256]{0,2,1:T(8,128)(2,1)}), bf16[128,8,256]{0,2,1:T(8,128)(2,1)S(1)}, u32[]{:S(2)}, u32[]{:S(2)}) async-start(bf16[128,8,256]{0,2,1:T(8,128)(2,1)} %pad_maximum_fusion), calls=%async_computation | async-start | bytes 1048576 | tf_op jit(solution)/shard_map/all_to_all | solution.py:361
  29.9 5.2 %copy-start.3 = (bf16[1,128,1024]{2,1,0:T(8,128)(2,1)S(1)}, bf16[1,128,1024]{2,1,0:T(8,128)(2,1)}, u32[]{:S(2)}) copy-start(bf16[1,128,1024]{2,1,0:T(8,128)(2,1)} %param.21) | copy-start | bytes 786436
  29.9 5.4 %copy-start.12 = (f32[1,128,2]{1,2,0:T(2,128)S(1)}, f32[1,128,2]{1,2,0:T(2,128)}, u32[]{:S(2)}) copy-start(f32[1,128,2]{1,2,0:T(2,128)} %param.36) | copy-start | bytes 3076
  31.4 12.7 %all-to-all-start.1 = ((bf16[8,2,8192]{2,1,0:T(2,128)(2,1)}), bf16[8,2,8192]{2,1,0:T(2,128)(2,1)S(1)}, u32[]{:S(2)}, u32[]{:S(2)}) async-start(bf16[8,2,8192]{2,1,0:T(2,128)(2,1)} %reshape.147), calls=%async_computation.1 | async-start | bytes 524288 | tf_op jit(solution)/shard_map/all_to_all | solution.py:398
  45.0 0.7 copy-start.8
  45.1 1.0 copy-start.2
  46.1 3.3 %copy-start.4 = (f32[2048]{0:T(1024)S(1)}, f32[2048]{0:T(1024)}, u32[]{:S(2)}) copy-start(f32[2048]{0:T(1024)} %param.34) | copy-start | bytes 24580
  46.1 3.3 %copy-start.5 = (f32[2048]{0:T(1024)S(1)}, f32[2048]{0:T(1024)}, u32[]{:S(2)}) copy-start(f32[2048]{0:T(1024)} %param.33) | copy-start | bytes 24580
  166.1 2.0 %copy-start.1 = (bf16[384,2048]{1,0:T(8,128)(2,1)S(1)}, bf16[384,2048]{1,0:T(8,128)(2,1)}, u32[]{:S(2)}) copy-start(bf16[384,2048]{1,0:T(8,128)(2,1)} %shard_map.190) | copy-start | bytes 4718596

commit v2 on v1

--- a/solution.py
+++ b/solution.py
@@ -110,7 +110,8 @@
     d = lax.axis_index("dp")
     nx = R // 2
     steps = S // group
-    order = [0] + list(range(steps - 1, 0, -1))
+    ahead = 2 // group
+    order = list(range(ahead)) + list(range(ahead, steps))
     members = [[p * group + i for i in range(group)] for p in order]
     width = wd.shape[1]
     ff = wg.shape[1]
@@ -250,14 +251,15 @@
             else:
                 ret_ref[pl.ds(0, cap), :] = total.astype(jnp.bfloat16)
 
-    arrive(0)
+    for p in range(ahead):
+        arrive(p)
     loads[0].wait()
     loads[1].wait()
     for p in range(steps):
         relay(p)
         gate_up(p)
-        if p + 1 < steps:
-            arrive(p + 1)
+        if p + ahead < steps:
+            arrive(p + ahead)
         if p == 0:
             loads[2].wait()
         if p > 1:
@@ -283,7 +285,7 @@
 def run_experts(outgoing, gate_w, up_w, down_w, S, R, cap):
     width, ff = gate_w.shape
     nx = R // 2
-    group = 2
+    group = 1
     bf = jnp.bfloat16
     dma = pltpu.SemaphoreType.DMA
     total = S * R * cap
@@ -396,9 +398,13 @@
         BLK,
     )
     returned_rows = lax.all_to_all(
-        outcome.astype(jnp.bfloat16), "sp", split_axis=0, concat_axis=1, tiled=True
-    )
-    blending_outcome = returned_rows.reshape(tok_rows, inner_width)
+        outcome.astype(jnp.bfloat16).reshape(sp_size, tok_rows, x_width),
+        "sp",
+        split_axis=0,
+        concat_axis=0,
+        tiled=True,
+    )
+    blending_outcome = jnp.concatenate([returned_rows[i] for i in range(sp_size)], axis=1)
     gated = blending_outcome.astype(jnp.float32) * jax.nn.silu(
         emitted_valve_unscaled[0].astype(jnp.float32)
     )

time: 170 us -> 157 us (0.924)
  the two profiles are of different devices: /device:TPU:0 before, /device:TPU:17 now
where the time goes in v2:
time: 157 us; the launch traced here: 156 us
  Pallas kernels  106 us (68%)
  waiting for transfers between devices  16.1 us (10%)
  starting transfers between devices  11.5 us (7%)
  matrix products  10.7 us (7%)
  local copies, waits for them, and re-layouts  7.14 us (5%)
  other arithmetic  4.09 us (3%)
    pallas_call x1, Pallas kernels, run_experts(): pl.pallas_call(functools.partial(expert_kernel, S, R, cap, group), out_sh...  106 us
    all_to_all x1, waiting for transfers between devices, per_device(): lax.all_to_all(payload.reshape(tok_rows, sp_size * sent_width), 'sp', spl...  9.37 us
    all_to_all x1, waiting for transfers between devices, per_device(): lax.all_to_all(outcome.astype(jnp.bfloat16).reshape(sp_size, tok_rows, x_...  6.76 us
    all_to_all x1, starting transfers between devices, per_device(): lax.all_to_all(outcome.astype(jnp.bfloat16).reshape(sp_size, tok_rows, x_...  5.94 us
    all_to_all x1, starting transfers between devices, per_device(): lax.all_to_all(payload.reshape(tok_rows, sp_size * sent_width), 'sp', spl...  5.61 us
    unnamed x41, local copies, waits for them, and re-layouts  3.73 us
    dot_general x2, matrix products, per_device(): jnp.dot(picking, answered, preferred_element_type=jnp.float32)  3.41 us
  transfers between devices with their start and end apart: 2, of which 2 were waited for; matrix products, arithmetic and copies ran while one was open for 2% of the time, Pallas kernels for 0%

profile of v2, /device:TPU:17, one launch (start us, length us, event | category | flops | bytes accessed | tf_op | source)
XLA Modules:
  0.0 156.3 jit_solution(1597718533847358438)
XLA Ops:
  0.0 1.2 copy.90
  1.2 1.0 copy.91
  2.2 1.0 copy.92
  3.2 0.8 pad_maximum_fusion
  4.0 5.6 %all-to-all-start = ((bf16[128,8,256]{0,2,1:T(8,128)(2,1)}), bf16[128,8,256]{0,2,1:T(8,128)(2,1)S(1)}, u32[]{:S(2)}, u32[]{:S(2)}) async-start(bf16[128,8,256]{0,2,1:T(8,128)(2,1)} %pad_maximum_fusion), calls=%async_computation | async-start | bytes 1048576 | tf_op jit(solution)/shard_map/all_to_all | solution.py:363
  9.8 0.6 reduce_window_sum.35
  11.0 0.6 reduce-window.6
  12.6 9.4 %all-to-all-done = bf16[128,8,256]{0,2,1:T(8,128)(2,1)S(1)} async-done(((bf16[128,8,256]{0,2,1:T(8,128)(2,1)}), bf16[128,8,256]{0,2,1:T(8,128)(2,1)S(1)}, u32[]{:S(2)}, u32[]{:S(2)}) %all-to-all-start) | async-done | bytes 524320 | tf_op jit(solution)/shard_map/all_to_all | solution.py:363
  22.3 0.6 multiply_convert_fusion
  23.7 0.3 fusion.34
  24.0 0.9 fusion.6
  24.8 0.4 fusion.8
  25.3 0.8 fusion.9
  26.1 0.9 copy.106
  27.0 5.9 %all-to-all-start.1 = ((bf16[8,128,128]{2,1,0:T(8,128)(2,1)}), bf16[8,128,128]{2,1,0:T(8,128)(2,1)S(1)}, u32[]{:S(2)}, u32[]{:S(2)}) async-start(bf16[8,128,128]{2,1,0:T(8,128)(2,1)} %copy.106), calls=%async_computation.1 | async-start | bytes 524288 | tf_op jit(solution)/shard_map/all_to_all | solution.py:400
  33.2 6.8 %all-to-all-done.1 = bf16[8,128,128]{2,1,0:T(8,128)(2,1)S(1)} async-done(((bf16[8,128,128]{2,1,0:T(8,128)(2,1)}), bf16[8,128,128]{2,1,0:T(8,128)(2,1)S(1)}, u32[]{:S(2)}, u32[]{:S(2)}) %all-to-all-start.1) | async-done | bytes 262176 | tf_op jit(solution)/shard_map/all_to_all | solution.py:400
  40.4 0.4 fusion.32
  41.1 0.2 copy-done.11
  41.4 3.1 %fusion.82 = (f32[128]{0:T(128)S(1)}, f32[128,2048]{1,0:T(8,128)S(1)}) fusion(bf16[1024,2048]{1,0:T(8,128)(2,1)} %param.32, f32[128,1024]{1,0:T(8,128)S(1)} %bitcast.173, f32[1024]{0:T(1024)S(1)} %copy-done.12, bf16[1,128,1024]{2,1,0:T(8,128)(2,1)S(1)} %copy-done.2, bf16[128,1024]{1,0:T(8,128)(2,1)S(1)} %fusion.53, bf16[1,128,2048]{2,1,0:T(8,128)(2,1)S(1)} %copy-done.11), kind=kOutput, calls=%fused_computation.137 | convolution fusion | flops 538967936 | bytes 6820352 | tf_op jit(solution)/shard_map/dot_general | solution.py:416
  44.5 0.3 multiply_reduce_fusion
  44.8 1.8 %convolution_convert_fusion.out_ref = bf16[384,2048]{1,0:T(8,128)(2,1)} fusion(s32[128]{0:T(128)S(1)} %get-tuple-element.18, s32[128]{0:T(128)S(1)} %get-tuple-element.17, f32[128,2048]{1,0:T(8,128)S(1)} %get-tuple-element.20, f32[2048]{0:T(1024)S(1)} %copy-done.3, f32[2048]{0:T(1024)S(1)} %copy-done.4, f32[128]{0:T(128)S(1)} %add_rsqrt_fusion.1, ...), kind=kOutput, calls=%fused_computation | convolution fusion | flops 203571200 | bytes 2639872 | tf_op jit(solution)/shard_map/dot_general | solution.py:435
  46.6 106.2 %shard_map.190 = bf16[384,2048]{1,0:T(8,128)(2,1)} custom-call(bf16[384,2048]{1,0:T(8,128)(2,1)} %convolution_convert_fusion.out_ref, bf16[2048,1280]{1,0:T(8,128)(2,1)} %bitcast.187, bf16[2048,1280]{1,0:T(8,128)(2,1)} %bitcast.188, bf16[1280,2048]{1,0:T(8,128)(2,1)} %bitcast.189), custom_call_target="tpu_custom_call" | custom-call | flops 24159191040 | bytes 15728640 | tf_op jit(solution)/shard_map/pallas_call | solution.py:292
  152.9 2.0 %convolution_multiply_fusion.1 = f32[128,2048]{1,0:T(8,128)S(1)} fusion(bf16[384,2048]{1,0:T(8,128)(2,1)} %shard_map.190, f32[128]{0:T(128)S(1)} %get-tuple-element.16, s32[128]{0:T(128)S(1)} %get-tuple-element.17), kind=kOutput, calls=%fused_computation.4 | convolution fusion | flops 201637888 | bytes 2622464 | tf_op jit(solution)/shard_map/dot_general | solution.py:449
  154.9 1.4 fusion.3
  (82 shorter events, 3.7 us)
Async XLA Ops:
  0.0 12.4 %copy-start = (f32[4,1024]{1,0:T(4,128)S(1)}, f32[4,1024]{1,0:T(4,128)}, u32[]{:S(2)}) copy-start(f32[4,1024]{1,0:T(4,128)} %param.28) | copy-start | bytes 49156
  0.0 9.6 %copy-start.13 = (f32[16]{0:T(128)S(1)}, f32[16]{0:T(128)}, u32[]{:S(2)}) copy-start(f32[16]{0:T(128)} %param.27) | copy-start | bytes 196
  0.0 9.7 %copy-start.5 = (f32[1,1024,2]{1,2,0:T(2,128)S(1)}, f32[1,1024,2]{1,2,0:T(2,128)}, u32[]{:S(2)}) copy-start(f32[1,1024,2]{1,2,0:T(2,128)} %param.25) | copy-start | bytes 24580
  0.0 9.7 %copy-start.6 = (f32[1,1024,2]{1,2,0:T(2,128)S(1)}, f32[1,1024,2]{1,2,0:T(2,128)}, u32[]{:S(2)}) copy-start(f32[1,1024,2]{1,2,0:T(2,128)} %param.26) | copy-start | bytes 24580
  0.0 10.5 %copy-start.7 = (s32[1,128,2]{1,2,0:T(2,128)S(1)}, s32[1,128,2]{1,2,0:T(2,128)}, u32[]{:S(2)}) copy-start(s32[1,128,2]{1,2,0:T(2,128)} %param.35) | copy-start | bytes 3076
  3.1 9.3 %copy-start.8 = (f32[4,256]{1,0:T(4,128)S(1)}, f32[4,256]{1,0:T(4,128)}, u32[]{:S(2)}) copy-start(f32[4,256]{1,0:T(4,128)} %param.30) | copy-start | bytes 12292
  3.1 9.3 %copy-start.9 = (f32[4,256]{1,0:T(4,128)S(1)}, f32[4,256]{1,0:T(4,128)}, u32[]{:S(2)}) copy-start(f32[4,256]{1,0:T(4,128)} %param.29) | copy-start | bytes 12292
  4.0 18.0 %all-to-all-start = ((bf16[128,8,256]{0,2,1:T(8,128)(2,1)}), bf16[128,8,256]{0,2,1:T(8,128)(2,1)S(1)}, u32[]{:S(2)}, u32[]{:S(2)}) async-start(bf16[128,8,256]{0,2,1:T(8,128)(2,1)} %pad_maximum_fusion), calls=%async_computation | async-start | bytes 1048576 | tf_op jit(solution)/shard_map/all_to_all | solution.py:363
  25.3 7.7 %copy-start.2 = (bf16[1,128,1024]{2,1,0:T(8,128)(2,1)S(1)}, bf16[1,128,1024]{2,1,0:T(8,128)(2,1)}, u32[]{:S(2)}) copy-start(bf16[1,128,1024]{2,1,0:T(8,128)(2,1)} %param.21) | copy-start | bytes 786436
  25.3 7.9 %copy-start.10 = (f32[1,128,2]{1,2,0:T(2,128)S(1)}, f32[1,128,2]{1,2,0:T(2,128)}, u32[]{:S(2)}) copy-start(f32[1,128,2]{1,2,0:T(2,128)} %param.36) | copy-start | bytes 3076
  27.0 13.0 %all-to-all-start.1 = ((bf16[8,128,128]{2,1,0:T(8,128)(2,1)}), bf16[8,128,128]{2,1,0:T(8,128)(2,1)S(1)}, u32[]{:S(2)}, u32[]{:S(2)}) async-start(bf16[8,128,128]{2,1,0:T(8,128)(2,1)} %copy.106), calls=%async_computation.1 | async-start | bytes 524288 | tf_op jit(solution)/shard_map/all_to_all | solution.py:400
  40.3 1.0 copy-start.11
  40.3 1.0 copy-start.12
  41.4 3.4 %copy-start.3 = (f32[2048]{0:T(1024)S(1)}, f32[2048]{0:T(1024)}, u32[]{:S(2)}) copy-start(f32[2048]{0:T(1024)} %param.34) | copy-start | bytes 24580
  41.4 3.4 %copy-start.4 = (f32[2048]{0:T(1024)S(1)}, f32[2048]{0:T(1024)}, u32[]{:S(2)}) copy-start(f32[2048]{0:T(1024)} %param.33) | copy-start | bytes 24580
  152.9 2.0 %copy-start.1 = (bf16[384,2048]{1,0:T(8,128)(2,1)S(1)}, bf16[384,2048]{1,0:T(8,128)(2,1)}, u32[]{:S(2)}) copy-start(bf16[384,2048]{1,0:T(8,128)(2,1)} %shard_map.190) | copy-start | bytes 4718596
